TPU v7x, 256 devices: a 4x2x16 block of a 4x16x16 slice. The times are simulated.
256 devices in a mesh: grp: 2 (over y), ep: 64 (over z, x), tp: 2 (over core).
Axes of the slice: x: 4, y: 2, z: 16, core: 2. Of those that a mesh axis runs over, the one named last changes fastest.
The devices are a block of a 4x16x16 slice.
Arguments:
- tokens: bfloat16 [32768, 2048], P(('grp', 'ep', 'tp')), parts along dimension 0, may hold values from -6 to 6
- norm_gain: float32 [2048], replicated, may hold values from 0.1 to 1.9
- expert_ids: int32 [32768, 2], P(('grp', 'ep', 'tp')), parts along dimension 0, may hold values from 0 to 31, all different within a row; in each aligned block of 128 rows (0 to 127, 128 to 255, ...) at most 10 rows name the same one
- route_weights: float32 [32768, 2], P(('grp', 'ep', 'tp')), parts along dimension 0, may hold values from 0.1 to 0.9
- w_gate: bfloat16 [2048, 114688], P(None, ('ep', 'tp')), may hold values from -0.125 to 0.125
- w_up: bfloat16 [2048, 114688], P(None, ('ep', 'tp')), may hold values from -0.125 to 0.125
- w_down: bfloat16 [114688, 2048], P(('ep', 'tp')), may hold values from -0.09375 to 0.09375
Outputs:
- mixed_out: bfloat16 [32768, 2048], P(('grp', 'ep', 'tp')), parts along dimension 0
There are 2 independent parts, one for each index of `grp`. A program takes and returns all parts, laid end to end along the dimension named above; an argument that names none is the same for every part. Nothing has to cross between parts.
Inputs may be any that keep to these rules, and one draw needn't show every extreme that they name: `expert_ids`: each row names 2 different experts. Among the rows of one device no expert is named more than 10 times, and in every draw some expert is named exactly 10 times by one device's rows.
All inputs are finite; a program needn't handle non-finite values.
Results may differ from a plain program's by a relative error of at most 0.01.
Values may be sent and summed in bfloat16 or wider, within the bound.
No kernel may reach another device: no remote copies, remote signals or barrier semaphores. Data moves between devices by JAX's collectives and lax.ppermute only.
A program may use at most 128 MiB of HBM per device.

v0:
```python
import jax
import jax.numpy as jnp
from jax import lax
from jax.sharding import PartitionSpec as P


def split_up(shard, dim, devices):
    before, after = (shard.shape[:dim], shard.shape[dim + 1 :])
    return jnp.moveaxis(shard.reshape(*before, devices, -1, *after), dim, 0)


def sum_at_owner(shard, axis, dim):
    devices = lax.axis_size(axis)
    blocks = lax.all_to_all(split_up(shard, dim, devices), axis, 0, 0, tiled=True)
    return jnp.sum(blocks.astype(jnp.float32), axis=0)


def partner_2(block, axis, apart):
    count = lax.axis_size(axis)
    route = []
    for low in range(count):
        high = low | 1 << apart
        if high != low and high < count:
            route += [(low, high), (high, low)]
    return lax.ppermute(block, axis, route)


def local(tokens, norm_gain, expert_ids, route_weights, w_gate, w_up, w_down):
    ep_count = lax.axis_size("ep")
    core_count = lax.axis_size("tp")
    expert_count = ep_count // 2
    tok_count = tokens.shape[0]
    model_width = tokens.shape[1]
    top_count = expert_ids.shape[1]
    capacity = 2 * max(1, 5 * tok_count * top_count // (8 * expert_count))
    source = lax.axis_index("ep") * core_count + lax.axis_index("tp")
    values = tokens.astype(jnp.float32)
    scale_rows = lax.rsqrt(jnp.mean(values * values, axis=1, keepdims=True) + 1e-06)
    normed = (values * scale_rows * norm_gain).astype(jnp.bfloat16)
    flat_ids = expert_ids.reshape(-1)
    route_count = flat_ids.shape[0]
    onehot = (flat_ids[:, None] == jnp.arange(expert_count, dtype=jnp.int32)[None, :]).astype(
        jnp.int32
    )
    earlier = jnp.cumsum(onehot, axis=0) - onehot
    slot_base = jnp.sum(earlier * onehot, axis=1)
    slot_index = jnp.remainder(slot_base + source, capacity)
    position = flat_ids * capacity + slot_index
    token_index = jnp.arange(route_count, dtype=jnp.int32) // top_count
    slot_table = (
        jnp.full((expert_count * capacity,), tok_count, jnp.int32).at[position].set(token_index)
    )
    padded = jnp.concatenate([normed, jnp.zeros((1, model_width), jnp.bfloat16)], axis=0)
    buffer = padded[slot_table].reshape(expert_count, capacity, model_width)
    half_slots = capacity // 2
    outgoing = buffer.reshape(ep_count, half_slots, model_width)
    arrived = lax.all_to_all(outgoing, "ep", split_axis=0, concat_axis=0, tiled=True).reshape(
        -1, model_width
    )
    partner = partner_2(arrived, "ep", 0)
    block_rows = lax.all_gather(
        jnp.concatenate([arrived, partner], axis=0), "tp", axis=0, tiled=True
    )
    gate_part = jnp.dot(block_rows, w_gate, preferred_element_type=jnp.float32)
    up_part = jnp.dot(block_rows, w_up, preferred_element_type=jnp.float32)
    hidden = (jax.nn.silu(gate_part) * up_part).astype(jnp.bfloat16)
    halves = sum_at_owner(
        jnp.dot(hidden, w_down, preferred_element_type=jnp.float32).astype(jnp.bfloat16), "tp", 0
    ).astype(jnp.bfloat16)
    own_rows = arrived.shape[0]
    partner_sums = partner_2(halves[own_rows:], "ep", 0)
    combined = (halves[:own_rows].astype(jnp.float32) + partner_sums.astype(jnp.float32)).astype(
        jnp.bfloat16
    )
    returned = lax.all_to_all(
        combined.reshape(ep_count, half_slots, model_width),
        "ep",
        split_axis=0,
        concat_axis=0,
        tiled=True,
    )
    summed = returned.reshape(expert_count, capacity, model_width).astype(jnp.float32)
    picked = summed.reshape(-1, model_width)[position].reshape(tok_count, top_count, model_width)
    mixed_out = jnp.sum(picked * route_weights[:, :, None], axis=1)
    return mixed_out.astype(jnp.bfloat16)


def solution(mesh):
    placed = (
        P(("grp", "ep", "tp"), None),
        P(),
        P(("grp", "ep", "tp"), None),
        P(("grp", "ep", "tp"), None),
        P(None, ("ep", "tp")),
        P(None, ("ep", "tp")),
        P(("ep", "tp"), None),
    )
    return jax.shard_map(
        local, mesh=mesh, in_specs=placed, out_specs=P(("grp", "ep", "tp"), None), check_vma=False
    )
```

profile of v0, /device:TPU:34, one launch (start us, length us, event | category | flops | bytes accessed | tf_op | source)
XLA Modules:
  0.0 411.0 jit_solution(868617568506192977)
XLA Ops:
  6.6 0.8 copy.10
  9.5 1.4 scatter_custom_fusion
  11.0 1.2 fusion.1
  12.2 1.2 fusion.3
  13.5 2.4 gather_fusion
  16.5 127.6 %all_to_all.15 = bf16[64,5,2048]{2,1,0:T(8,128)(2,1)} all-to-all(bf16[64,5,2048]{2,1,0:T(8,128)(2,1)S(1)} %reshape_reshape.3), channel_id=1, replica_groups=mesh['grp'=2,'ep'=64,'tp'=2] {'ep'}, dimensions={0} | all-to-all | bytes 2621440 | tf_op jit(solution)/shard_map/all_to_all | solution.py:57
  144.1 2.6 reshape.99
  147.4 26.9 %collective-permute-done = bf16[320,2048]{1,0:T(8,128)(2,1)S(1)} collective-permute-done((bf16[320,2048]{1,0:T(8,128)(2,1)S(1)}, bf16[320,2048]{1,0:T(8,128)(2,1)S(1)}, u32[]{:S(2)}, u32[]{:S(2)}) %collective-permute-start) | collective-permute-done | bytes 1310752 | tf_op jit(solution)/shard_map/ppermute | solution.py:25
  174.3 1.8 pad_maximum_fusion
  176.1 19.2 %all-gather.2.cloned.1.call-done = bf16[1280,2048]{1,0:T(8,128)(2,1)} async-done(((bf16[640,2048]{1,0:T(8,128)(2,1)}), bf16[1280,2048]{1,0:T(8,128)(2,1)}) %all-gather.2.cloned.1.call-update) | async-done | bytes 5242896 | tf_op jit(solution)/shard_map/all_gather | solution.py:61
  195.4 10.0 %fusion.14 = f32[1280,896]{1,0:T(8,128)} fusion(bf16[1280,2048]{1,0:T(8,128)(2,1)} %all-gather.2.cloned.1.call-done, bf16[2048,896]{1,0:T(8,128)(2,1)} %param.11), kind=kOutput, calls=%fused_computation.40 | convolution fusion | flops 4697620480 | bytes 13500416 | tf_op jit(solution)/shard_map/dot_general | solution.py:64
  205.4 17.6 %convolution_convert_fusion = bf16[1280,2048]{1,0:T(8,128)(2,1)} fusion(bf16[896,2048]{1,0:T(8,128)(2,1)} %param.13, f32[1280,896]{1,0:T(8,128)} %fusion.14, bf16[1280,2048]{1,0:T(8,128)(2,1)} %all-gather.2.cloned.1.call-done, bf16[2048,896]{1,0:T(8,128)(2,1)} %param.12), kind=kOutput, calls=%fused_computation.3 | convolution fusion | flops 9404743680 | bytes 22413312 | tf_op jit(solution)/shard_map/dot_general | solution.py:68
  222.9 13.8 %all_to_all.16 = bf16[2,640,2048]{2,1,0:T(8,128)(2,1)} all-to-all(bf16[2,640,2048]{2,1,0:T(8,128)(2,1)} %bitcast.27), channel_id=1, replica_groups=mesh['grp'=2,'ep'=64,'tp'=2] {'tp'}, dimensions={0} | all-to-all | bytes 10485760 | tf_op jit(solution)/shard_map/all_to_all | solution.py:14
  236.7 4.3 %reduce_sum.41 = bf16[640,2048]{1,0:T(8,128)(2,1)S(1)} reduce(bf16[2,640,2048]{2,1,0:T(8,128)(2,1)} %all_to_all.16, bf16[]{:T(256)} %constant.51.clone.1), dimensions={0}, to_apply=%region_5.6 | reduce | flops 1310720 | bytes 7864322 | tf_op jit(solution)/shard_map/reduce_sum | solution.py:15
  241.2 1.4 collective-permute-start.1
  242.5 29.6 %collective-permute-done.1 = bf16[320,2048]{1,0:T(8,128)(2,1)S(1)} collective-permute-done((bf16[320,2048]{1,0:T(8,128)(2,1)S(1)}, bf16[320,2048]{1,0:T(8,128)(2,1)S(1)}, u32[]{:S(2)}, u32[]{:S(2)}) %collective-permute-start.1) | collective-permute-done | bytes 1310752 | tf_op jit(solution)/shard_map/ppermute | solution.py:25
  272.1 1.5 add_convert_fusion
  273.6 3.4 reshape.101
  277.0 16.4 %all-to-all-start.2 = ((bf16[64,5,2048]{2,1,0:T(8,128)(2,1)}), bf16[64,5,2048]{2,1,0:T(8,128)(2,1)}, u32[]{:S(2)}, u32[]{:S(2)}) async-start(bf16[64,5,2048]{2,1,0:T(8,128)(2,1)} %reshape.101), calls=%async_computation.2 | async-start | bytes 4194304 | tf_op jit(solution)/shard_map/all_to_all | solution.py:75
  293.6 99.0 %all-to-all-done.2 = bf16[64,5,2048]{2,1,0:T(8,128)(2,1)} async-done(((bf16[64,5,2048]{2,1,0:T(8,128)(2,1)}), bf16[64,5,2048]{2,1,0:T(8,128)(2,1)}, u32[]{:S(2)}, u32[]{:S(2)}) %all-to-all-start.2) | async-done | bytes 1310752 | tf_op jit(solution)/shard_map/all_to_all | solution.py:75
  392.5 2.5 reshape.103
  395.0 2.7 gather_fusion.1
  397.7 2.5 reshape.102
  400.2 3.9 multiply_reduce_fusion
  (27 shorter events, 3.7 us)
Async XLA Ops:
  6.5 188.8 %all-gather.2.cloned.1.call-start = ((), (), s32[]{:S(2)}) async-start(), calls=%async_computation.3 | async-start | bytes 7864320 | tf_op jit(solution)/shard_map/all_gather | solution.py:61
  146.7 27.6 %collective-permute-start = (bf16[320,2048]{1,0:T(8,128)(2,1)S(1)}, bf16[320,2048]{1,0:T(8,128)(2,1)S(1)}, u32[]{:S(2)}, u32[]{:S(2)}) collective-permute-start(bf16[320,2048]{1,0:T(8,128)(2,1)S(1)} %reshape.99), channel_id=1, source_target_pairs={{0,2},{2,0},{4,6},{6,4},{8,10},{10,8},{12,14},{14,12},{16,18},{18,... | collective-permute-start | bytes 3932168 | tf_op jit(solution)/shard_map/ppermute | solution.py:25
  241.2 30.9 %collective-permute-start.1 = (bf16[320,2048]{1,0:T(8,128)(2,1)S(1)}, bf16[320,2048]{1,0:T(8,128)(2,1)S(1)}, u32[]{:S(2)}, u32[]{:S(2)}) collective-permute-start(bf16[320,2048]{1,0:T(8,128)(2,1)S(1)} %slice.22), channel_id=1, source_target_pairs={{0,2},{2,0},{4,6},{6,4},{8,10},{10,8},{12,14},{14,12},{16,18},{18,... | collective-permute-start | bytes 3932168 | tf_op jit(solution)/shard_map/ppermute | solution.py:25
  273.6 19.8 %copy-start = (f32[128,2]{0,1:T(2,128)S(1)}, f32[128,2]{0,1:T(2,128)}, u32[]{:S(2)}) copy-start(f32[128,2]{0,1:T(2,128)} %param.10) | copy-start | bytes 3076
  277.0 115.5 %all-to-all-start.2 = ((bf16[64,5,2048]{2,1,0:T(8,128)(2,1)}), bf16[64,5,2048]{2,1,0:T(8,128)(2,1)}, u32[]{:S(2)}, u32[]{:S(2)}) async-start(bf16[64,5,2048]{2,1,0:T(8,128)(2,1)} %reshape.101), calls=%async_computation.2 | async-start | bytes 4194304 | tf_op jit(solution)/shard_map/all_to_all | solution.py:75
Sparse Core Ops, SparseCore 0:
  176.3 19.0 all-gather.1
where the time goes:
time: 412 us; the launch traced here: 411 us
  waiting for transfers between devices  175 us (42%)
  blocking collectives  141 us (34%)
  matrix products  27.5 us (7%)
  local copies, waits for them, and re-layouts  19.8 us (5%)
  starting transfers between devices  18.4 us (4%)
  other arithmetic  15.5 us (4%)
  between operations  13.6 us (3%)
    all_to_all x1, blocking collectives, local(): lax.all_to_all(outgoing, 'ep', split_axis=0, concat_axis=0, tiled=True)  128 us
    all_to_all x1, waiting for transfers between devices, local(): lax.all_to_all(combined.reshape(ep_count, half_slots, model_width), 'ep',...  99 us
    ppermute x2, waiting for transfers between devices, partner_2(): return lax.ppermute(block, axis, route)  56.5 us
    all_gather x1, waiting for transfers between devices, local(): lax.all_gather(jnp.concatenate([arrived, partner], axis=0), 'tp', axis=0,...  19.2 us
    dot_general x1, matrix products, local(): jnp.dot(hidden, w_down, preferred_element_type=jnp.float32)  17.6 us
    all_to_all x1, starting transfers between devices, local(): lax.all_to_all(combined.reshape(ep_count, half_slots, model_width), 'ep',...  16.4 us
    all_to_all x1, blocking collectives, sum_at_owner(): lax.all_to_all(split_up(shard, dim, devices), axis, 0, 0, tiled=True)  13.8 us
    dot_general x1, matrix products, local(): gate_part = jnp.dot(block_rows, w_gate, preferred_element_type=jnp.float32)  9.98 us
  transfers between devices with their start and end apart: 4, of which 4 were waited for; matrix products, arithmetic and copies ran while one was open for 0% of the time, Pallas kernels for 0%

commit v1 on v0

--- a/solution.py
+++ b/solution.py
@@ -2,6 +2,7 @@
 import jax.numpy as jnp
 from jax import lax
 from jax.sharding import PartitionSpec as P
+from jax.lax import all_to_all, axis_size
 
 
 def split_up(shard, dim, devices):
@@ -58,8 +59,15 @@
         -1, model_width
     )
     partner = partner_2(arrived, "ep", 0)
-    block_rows = lax.all_gather(
-        jnp.concatenate([arrived, partner], axis=0), "tp", axis=0, tiled=True
+    block_in = jnp.concatenate([arrived, partner], axis=0)
+    block_rows = jnp.concatenate(
+        all_to_all(
+            jnp.stack([block_in for _ in range(axis_size("tp"))]),
+            axis_name="tp",
+            split_axis=0,
+            concat_axis=0,
+        ),
+        axis=0,
     )
     gate_part = jnp.dot(block_rows, w_gate, preferred_element_type=jnp.float32)
     up_part = jnp.dot(block_rows, w_up, preferred_element_type=jnp.float32)

time: 412 us -> 379 us (0.920)
  waiting for transfers between devices: 175 us -> 156 us
  between operations: 13.6 us -> 0.19 us
  blocking collectives: 141 us -> 149 us
  starting transfers between devices: 18.4 us -> 10.6 us
    all_gather x1 -> x0, waiting for transfers between devices: 19.2 us -> none  [local(): lax.all_gather(jnp.concatenate([arrived, partner], axis=0), 'tp', axis=0,...]
    all_to_all x0 -> x1, blocking collectives: none -> 8.23 us  [local(): all_to_all(jnp.stack([block_in for _ in range(axis_size('tp'))]), axis_na...]
    all_to_all x1, starting transfers between devices: 16.4 us -> 9.49 us  [local(): lax.all_to_all(combined.reshape(ep_count, half_slots, model_width), 'ep',...]
  transfers between devices with their start and end apart: 4 -> 3, of which waited for: 4 -> 3; matrix products, arithmetic and copies ran while one was open for 0% -> 0% of each run, Pallas kernels for 0% -> 0%
where the time goes in v1:
time: 379 us; the launch traced here: 378 us
  waiting for transfers between devices  156 us (41%)
  blocking collectives  149 us (39%)
  matrix products  24.7 us (7%)
  local copies, waits for them, and re-layouts  22.2 us (6%)
  other arithmetic  14.5 us (4%)
  starting transfers between devices  10.6 us (3%)
    all_to_all x1, blocking collectives, local(): lax.all_to_all(outgoing, 'ep', split_axis=0, concat_axis=0, tiled=True)  128 us
    all_to_all x1, waiting for transfers between devices, local(): lax.all_to_all(combined.reshape(ep_count, half_slots, model_width), 'ep',...  98.9 us
    ppermute x2, waiting for transfers between devices, partner_2(): return lax.ppermute(block, axis, route)  57.4 us
    dot_general x1, matrix products, local(): jnp.dot(hidden, w_down, preferred_element_type=jnp.float32)  17.5 us
    all_to_all x1, blocking collectives, sum_at_owner(): lax.all_to_all(split_up(shard, dim, devices), axis, 0, 0, tiled=True)  13.6 us
    all_to_all x1, starting transfers between devices, local(): lax.all_to_all(combined.reshape(ep_count, half_slots, model_width), 'ep',...  9.49 us
    all_to_all x1, blocking collectives, local(): all_to_all(jnp.stack([block_in for _ in range(axis_size('tp'))]), axis_na...  8.23 us
  transfers between devices with their start and end apart: 3, of which 3 were waited for; matrix products, arithmetic and copies ran while one was open for 0% of the time, Pallas kernels for 0%

profile of v1, /device:TPU:34, one launch (start us, length us, event | category | flops | bytes accessed | tf_op | source)
XLA Modules:
  0.0 377.9 jit_solution(17306708712699962949)
XLA Ops:
  0.0 0.8 copy.10
  1.1 0.7 broadcast_multiply_fusion
  3.0 1.4 scatter_custom_fusion
  4.4 1.2 fusion
  5.7 1.2 fusion.2
  6.9 2.4 gather_fusion
  9.9 127.6 %all_to_all.20 = bf16[64,5,2048]{2,1,0:T(8,128)(2,1)} all-to-all(bf16[64,5,2048]{2,1,0:T(8,128)(2,1)S(1)} %reshape_reshape.3), channel_id=1, replica_groups=mesh['grp'=2,'ep'=64,'tp'=2] {'ep'}, dimensions={0} | all-to-all | bytes 2621440 | tf_op jit(solution)/shard_map/all_to_all | solution.py:58
  137.6 2.6 reshape.102
  140.8 26.9 %collective-permute-done = bf16[320,2048]{1,0:T(8,128)(2,1)S(1)} collective-permute-done((bf16[320,2048]{1,0:T(8,128)(2,1)S(1)}, bf16[320,2048]{1,0:T(8,128)(2,1)S(1)}, u32[]{:S(2)}, u32[]{:S(2)}) %collective-permute-start) | collective-permute-done | bytes 1310752 | tf_op jit(solution)/shard_map/ppermute | solution.py:26
  168.5 8.2 %all_to_all.21 = bf16[2,640,2048]{2,1,0:T(8,128)(2,1)S(1)} all-to-all(bf16[2,640,2048]{2,1,0:T(8,128)(2,1)S(1)} %pad_maximum_fusion), channel_id=1, replica_groups=mesh['grp'=2,'ep'=64,'tp'=2] {'tp'}, dimensions={0} | all-to-all | bytes 10485760 | tf_op jit(solution)/shard_map/all_to_all | solution.py:64
  176.8 2.3 copy-done
  179.1 7.1 %fusion.11 = f32[1280,896]{1,0:T(8,128)} fusion(bf16[1280,2048]{1,0:T(8,128)(2,1)S(1)} %bitcast.30, bf16[2048,896]{1,0:T(8,128)(2,1)S(1)} %copy-done.2), kind=kOutput, calls=%fused_computation.39 | convolution fusion | flops 4697620480 | bytes 13500416 | tf_op jit(solution)/shard_map/dot_general | solution.py:72
  186.3 17.5 %convolution_convert_fusion = bf16[1280,2048]{1,0:T(8,128)(2,1)} fusion(bf16[896,2048]{1,0:T(8,128)(2,1)} %param.13, f32[1280,896]{1,0:T(8,128)} %fusion.11, bf16[1280,2048]{1,0:T(8,128)(2,1)} %bitcast.31, bf16[2048,896]{1,0:T(8,128)(2,1)} %param.12), kind=kOutput, calls=%fused_computation.3 | convolution fusion | flops 9404743680 | bytes 22413312 | tf_op jit(solution)/shard_map/dot_general | solution.py:76
  203.8 13.6 %all_to_all.22 = bf16[2,640,2048]{2,1,0:T(8,128)(2,1)} all-to-all(bf16[2,640,2048]{2,1,0:T(8,128)(2,1)} %bitcast.32), channel_id=1, replica_groups=mesh['grp'=2,'ep'=64,'tp'=2] {'tp'}, dimensions={0} | all-to-all | bytes 10485760 | tf_op jit(solution)/shard_map/all_to_all | solution.py:15
  217.4 4.3 %reduce_sum.41 = bf16[640,2048]{1,0:T(8,128)(2,1)S(1)} reduce(bf16[2,640,2048]{2,1,0:T(8,128)(2,1)} %all_to_all.22, bf16[]{:T(256)} %constant.51.clone.1), dimensions={0}, to_apply=%region_5.6 | reduce | flops 1310720 | bytes 7864322 | tf_op jit(solution)/shard_map/reduce_sum | solution.py:16
  222.3 30.5 %collective-permute-done.1 = bf16[320,2048]{1,0:T(8,128)(2,1)S(1)} collective-permute-done((bf16[320,2048]{1,0:T(8,128)(2,1)S(1)}, bf16[320,2048]{1,0:T(8,128)(2,1)S(1)}, u32[]{:S(2)}, u32[]{:S(2)}) %collective-permute-start.1) | collective-permute-done | bytes 1310752 | tf_op jit(solution)/shard_map/ppermute | solution.py:26
  252.8 1.5 add_convert_fusion
  254.3 3.4 reshape.105
  257.7 9.5 %all-to-all-start.3 = ((bf16[64,5,2048]{2,1,0:T(8,128)(2,1)}), bf16[64,5,2048]{2,1,0:T(8,128)(2,1)}, u32[]{:S(2)}, u32[]{:S(2)}) async-start(bf16[64,5,2048]{2,1,0:T(8,128)(2,1)} %reshape.105), calls=%async_computation.3 | async-start | bytes 4194304 | tf_op jit(solution)/shard_map/all_to_all | solution.py:83
  267.3 98.9 %all-to-all-done.3 = bf16[64,5,2048]{2,1,0:T(8,128)(2,1)} async-done(((bf16[64,5,2048]{2,1,0:T(8,128)(2,1)}), bf16[64,5,2048]{2,1,0:T(8,128)(2,1)}, u32[]{:S(2)}, u32[]{:S(2)}) %all-to-all-start.3) | async-done | bytes 1310752 | tf_op jit(solution)/shard_map/all_to_all | solution.py:83
  366.3 2.5 reshape.107
  368.8 2.7 gather_fusion.1
  371.5 2.5 reshape.106
  374.0 3.9 %multiply_reduce_fusion = bf16[128,2048]{1,0:T(8,128)(2,1)} fusion(f32[128,2,2048]{2,1,0:T(2,128)S(1)} %reshape.106, f32[128,2]{1,0:T(8,128)S(1)} %copy.13), kind=kLoop, calls=%fused_computation.8 | loop fusion | flops 786432 | bytes 2622464 | tf_op jit(solution)/shard_map/reduce_sum | solution.py:92
  (30 shorter events, 4.2 us)
Async XLA Ops:
  140.2 27.6 %collective-permute-start = (bf16[320,2048]{1,0:T(8,128)(2,1)S(1)}, bf16[320,2048]{1,0:T(8,128)(2,1)S(1)}, u32[]{:S(2)}, u32[]{:S(2)}) collective-permute-start(bf16[320,2048]{1,0:T(8,128)(2,1)S(1)} %reshape.102), channel_id=1, source_target_pairs={{0,2},{2,0},{4,6},{6,4},{8,10},{10,8},{12,14},{14,12},{16,18},{18,... | collective-permute-start | bytes 3932168 | tf_op jit(solution)/shard_map/ppermute | solution.py:26
  168.5 10.6 %copy-start.2 = (bf16[2048,896]{1,0:T(8,128)(2,1)S(1)}, bf16[2048,896]{1,0:T(8,128)(2,1)}, u32[]{:S(2)}) copy-start(bf16[2048,896]{1,0:T(8,128)(2,1)} %param.11) | copy-start | bytes 11010052
  176.8 2.3 copy-start
  221.8 30.9 %collective-permute-start.1 = (bf16[320,2048]{1,0:T(8,128)(2,1)S(1)}, bf16[320,2048]{1,0:T(8,128)(2,1)S(1)}, u32[]{:S(2)}, u32[]{:S(2)}) collective-permute-start(bf16[320,2048]{1,0:T(8,128)(2,1)S(1)} %slice.22), channel_id=1, source_target_pairs={{0,2},{2,0},{4,6},{6,4},{8,10},{10,8},{12,14},{14,12},{16,18},{18,... | collective-permute-start | bytes 3932168 | tf_op jit(solution)/shard_map/ppermute | solution.py:26
  254.3 12.9 %copy-start.1 = (f32[128,2]{0,1:T(2,128)S(1)}, f32[128,2]{0,1:T(2,128)}, u32[]{:S(2)}) copy-start(f32[128,2]{0,1:T(2,128)} %param.10) | copy-start | bytes 3076
  257.7 108.6 %all-to-all-start.3 = ((bf16[64,5,2048]{2,1,0:T(8,128)(2,1)}), bf16[64,5,2048]{2,1,0:T(8,128)(2,1)}, u32[]{:S(2)}, u32[]{:S(2)}) async-start(bf16[64,5,2048]{2,1,0:T(8,128)(2,1)} %reshape.105), calls=%async_computation.3 | async-start | bytes 4194304 | tf_op jit(solution)/shard_map/all_to_all | solution.py:83
